TPU v7x, 32 devices: a whole 2x2x4 slice. The times are simulated.
32 devices in a mesh: kv: 4 (over y, x), tp: 8 (over z, core).
Axes of the slice: x: 2, y: 2, z: 4, core: 2. Of those that a mesh axis runs over, the one named last changes fastest.
Arguments:
- tokens: bfloat16 [256, 4096], P(None, ('kv', 'tp')), may hold values from -10 to 10
- past_state: float32 [256, 32, 64, 128], P('kv', 'tp'), may hold values from -6 to 6
- first_gain: float32 [4096], P('kv'), may hold values from 0.1 to 1.9
- first_gate: bfloat16 [4096, 11264], P('kv', 'tp'), may hold values from -0.09375 to 0.09375
- first_up: bfloat16 [4096, 11264], P('kv', 'tp'), may hold values from -0.09375 to 0.09375
- first_down: bfloat16 [11264, 4096], P('tp', 'kv'), may hold values from -0.078125 to 0.078125
- mix_gain: float32 [4096], P('kv'), may hold values from 0.1 to 1.9
- query_weight: bfloat16 [4096, 2048], P('kv', 'tp'), may hold values from -0.09375 to 0.09375
- key_weight: bfloat16 [4096, 2048], P('kv', 'tp'), may hold values from -0.09375 to 0.09375
- value_weight: bfloat16 [4096, 4096], P('kv', 'tp'), may hold values from -0.09375 to 0.09375
- output_gate_weight: bfloat16 [4096, 4096], P('kv', 'tp'), may hold values from -0.09375 to 0.09375
- head_gain: float32 [4096], P('tp'), may hold values from 0.1 to 1.9
- out_weight: bfloat16 [4096, 4096], P('tp', 'kv'), may hold values from -0.125 to 0.125
- second_gain: float32 [4096], P('kv'), may hold values from 0.1 to 1.9
- second_gate: bfloat16 [4096, 11264], P('kv', 'tp'), may hold values from -0.09375 to 0.09375
- second_up: bfloat16 [4096, 11264], P('kv', 'tp'), may hold values from -0.09375 to 0.09375
- second_down: bfloat16 [11264, 4096], P('tp', 'kv'), may hold values from -0.078125 to 0.078125
Outputs:
- mixed: bfloat16 [256, 4096], P(None, ('kv', 'tp'))
- new_state: float32 [256, 32, 64, 128], P('kv', 'tp')
All inputs are finite; a program needn't handle non-finite values.
Results may differ from a plain program's by a relative error of at most 0.033.
Values may be sent and summed in bfloat16 or wider, within the bound.
A program may use at most 128 MiB of HBM per device.

v0:
```python
import jax
import jax.numpy as jnp
from jax import lax
from jax.sharding import PartitionSpec as P

D = 4096
HEADS = 32
HEAD_K = 64
HEAD_V = 128
POS = 16384


EPS_RMS = 1e-06
EPS_GROUP = 1e-05
ROPE_BASE = 10000.0


def rotate(vectors):
    half_width = vectors.shape[-1] // 2
    frequency = ROPE_BASE ** (-jnp.arange(half_width, dtype=jnp.float32) / half_width)
    angles = POS * frequency
    cosine = jnp.cos(angles)
    sine_part = jnp.sin(angles)
    lower = vectors[..., :half_width]
    upper = vectors[..., half_width:]
    return jnp.concatenate(
        [lower * cosine - upper * sine_part, lower * sine_part + upper * cosine], axis=-1
    )


def activate(gate_sum, up_sum, summed):
    inverse_rms = lax.rsqrt(summed / D + EPS_RMS)[:, None]
    return (jax.nn.silu(gate_sum * inverse_rms) * (up_sum * inverse_rms)).astype(jnp.bfloat16)


def channel_mix(widened, gain, w_gate, w_up, w_down):
    widened_f = widened.astype(jnp.float32)
    scaled = (widened_f * gain).astype(jnp.bfloat16)
    squares = jnp.sum(widened_f * widened_f, axis=1)
    gate_part = jnp.dot(scaled, w_gate, preferred_element_type=jnp.float32)
    up_part = jnp.dot(scaled, w_up, preferred_element_type=jnp.float32)
    gate_sum, up_sum, summed = (
        lax.psum(gate_part.astype(jnp.bfloat16), "kv").astype(jnp.float32),
        lax.psum(up_part.astype(jnp.bfloat16), "kv").astype(jnp.float32),
        lax.psum(squares.astype(jnp.bfloat16), "kv").astype(jnp.float32),
    )
    return 0.5 * jnp.dot(
        activate(gate_sum, up_sum, summed), w_down, preferred_element_type=jnp.float32
    )


def token_mix(
    widened,
    past_state,
    gain,
    query_weight,
    key_weight,
    value_weight,
    output_gate_weight,
    head_gain,
    out_weight,
):
    widened_f = widened.astype(jnp.float32)
    scaled = (widened_f * gain).astype(jnp.bfloat16)
    squares = jnp.sum(widened_f * widened_f, axis=1)
    query_part = jnp.dot(scaled, query_weight, preferred_element_type=jnp.float32)
    key_part = jnp.dot(scaled, key_weight, preferred_element_type=jnp.float32)
    value_part = jnp.dot(scaled, value_weight, preferred_element_type=jnp.float32)
    gate_part = jnp.dot(scaled, output_gate_weight, preferred_element_type=jnp.float32)
    queries, keys_now, values_now, gate_now, summed = (
        lax.psum_scatter(
            query_part.astype(jnp.bfloat16), "kv", scatter_dimension=0, tiled=True
        ).astype(jnp.float32),
        lax.psum_scatter(
            key_part.astype(jnp.bfloat16), "kv", scatter_dimension=0, tiled=True
        ).astype(jnp.float32),
        lax.psum_scatter(
            value_part.astype(jnp.bfloat16), "kv", scatter_dimension=0, tiled=True
        ).astype(jnp.float32),
        lax.psum_scatter(
            gate_part.astype(jnp.bfloat16), "kv", scatter_dimension=0, tiled=True
        ).astype(jnp.float32),
        lax.psum_scatter(
            squares.astype(jnp.bfloat16), "kv", scatter_dimension=0, tiled=True
        ).astype(jnp.float32),
    )
    inverse_rms = lax.rsqrt(summed / D + EPS_RMS)[:, None]
    row_count = past_state.shape[0]
    local_heads = past_state.shape[1]
    queries = rotate((queries * inverse_rms).reshape(row_count, local_heads, HEAD_K)) * HEAD_K ** (
        -0.5
    )
    keys_now = rotate((keys_now * inverse_rms).reshape(row_count, local_heads, HEAD_K))
    values_now = (values_now * inverse_rms).reshape(row_count, local_heads, HEAD_V)
    gate_now = gate_now * inverse_rms
    head_level = (lax.axis_index("tp") * local_heads + jnp.arange(local_heads)).astype(jnp.float32)
    retained = 1.0 - jnp.exp2(-5.0 - 16.0 * head_level / (HEADS - 1))
    new_state = (
        retained[None, :, None, None] * past_state
        + keys_now[:, :, :, None] * values_now[:, :, None, :]
    )
    retrieved = jnp.einsum("bhk,bhkv->bhv", queries, new_state, precision=lax.Precision.HIGHEST)
    head_mean = jnp.mean(retrieved, axis=-1, keepdims=True)
    variance = jnp.mean(jnp.square(retrieved - head_mean), axis=-1, keepdims=True)
    normed = ((retrieved - head_mean) * lax.rsqrt(variance + EPS_GROUP)).reshape(
        row_count, local_heads * HEAD_V
    )
    mixed_heads = (jax.nn.silu(gate_now) * (normed * head_gain)).astype(jnp.bfloat16)
    projected = jnp.dot(
        lax.all_gather(mixed_heads, "kv", axis=0, tiled=True),
        out_weight,
        preferred_element_type=jnp.float32,
    )
    return (projected, new_state)


def shards(
    tokens,
    past_state,
    first_gain,
    first_gate,
    first_up,
    first_down,
    mix_gain,
    query_weight,
    key_weight,
    value_weight,
    output_gate_weight,
    head_gain,
    out_weight,
    second_gain,
    second_gate,
    second_up,
    second_down,
):

    def first_section(widened):
        return (channel_mix(widened, first_gain, first_gate, first_up, first_down), None)

    def middle_section(widened):
        return token_mix(
            widened,
            past_state,
            mix_gain,
            query_weight,
            key_weight,
            value_weight,
            output_gate_weight,
            head_gain,
            out_weight,
        )

    def last_section(widened):
        return (channel_mix(widened, second_gain, second_gate, second_up, second_down), None)

    sections = [first_section, middle_section, last_section]
    own_columns = tokens
    widened = lax.all_gather(tokens, "tp", axis=1, tiled=True)
    state_out = past_state
    for section_index in range(3):
        branch_out, produced = sections[section_index](widened)
        if produced is not None:
            state_out = produced
        own_piece = lax.psum_scatter(
            branch_out.astype(jnp.bfloat16), "tp", scatter_dimension=1, tiled=True
        ).astype(jnp.float32)
        own_columns = (own_columns.astype(jnp.float32) + own_piece).astype(jnp.bfloat16)
        if section_index < 2:
            widened = lax.all_gather(own_columns, "tp", axis=1, tiled=True)
    return (own_columns, state_out)


def solution(mesh):
    in_specs = (
        P(None, ("kv", "tp")),
        P("kv", "tp", None, None),
        P("kv"),
        P("kv", "tp"),
        P("kv", "tp"),
        P("tp", "kv"),
        P("kv"),
        P("kv", "tp"),
        P("kv", "tp"),
        P("kv", "tp"),
        P("kv", "tp"),
        P("tp"),
        P("tp", "kv"),
        P("kv"),
        P("kv", "tp"),
        P("kv", "tp"),
        P("tp", "kv"),
    )
    out_specs = (P(None, ("kv", "tp")), P("kv", "tp", None, None))
    return jax.shard_map(shards, mesh=mesh, in_specs=in_specs, out_specs=out_specs, check_vma=False)
```

profile of v0, /device:TPU:0, one launch (start us, length us, event | category | flops | bytes accessed | tf_op | source)
XLA Modules:
  0.0 409.7 jit_solution(10858656113238108868)
XLA Ops:
  7.2 15.8 %all_gather.12 = bf16[256,1024]{1,0:T(8,128)(2,1)S(1)} all-gather(bf16[256,128]{1,0:T(8,128)(2,1)} %param.17), channel_id=1, replica_groups=mesh['kv'=4,'tp'=8] {'tp'}, dimensions={1}, use_global_device_ids=true | all-gather | bytes 589824 | tf_op jit(solution)/shard_map/all_gather | solution.py:158
  23.0 2.5 convolution_convert_fusion.2
  25.6 1.9 convolution_convert_fusion.3
  27.7 10.1 %psum.43 = bf16[256]{0:T(256)(128)(2,1)S(1)} all-reduce(bf16[256]{0:T(256)(128)(2,1)S(1)} %fusion.3), channel_id=1, replica_groups=mesh['kv'=4,'tp'=8] {'kv'}, use_global_device_ids=true, to_apply=%region_2.0 | all-reduce | flops 256 | bytes 1024 | tf_op jit(solution)/shard_map/psum | solution.py:45
  37.8 48.4 %all-reduce.8.cloned.1.call-done = (bf16[256,1408]{1,0:T(8,128)(2,1)}, bf16[256,1408]{1,0:T(8,128)(2,1)}) async-done(((bf16[256,1408]{1,0:T(8,128)(2,1)}, bf16[256,1408]{1,0:T(8,128)(2,1)}), (bf16[256,1408]{1,0:T(8,128)(2,1)}, bf16[256,1408]{1,0:T(8,128)(2,1)})) %all-reduce.8.cloned.1.call-update) | async-done | bytes 1441808 | tf_op jit(solution)/shard_map/psum | solution.py:44
  86.2 3.5 fusion
  89.7 1.0 copy.24
  90.8 31.2 %reduce-scatter.22.cloned.1.call-done = bf16[128,256]{1,0:T(8,128)(2,1)} async-done(((bf16[1024,256]{1,0:T(8,128)(2,1)}), bf16[128,256]{1,0:T(8,128)(2,1)}) %reduce-scatter.22.cloned.1.call-update) | async-done | bytes 65552
  123.0 14.0 %all_gather.13 = bf16[256,1024]{1,0:T(8,128)(2,1)S(1)} all-gather(bf16[256,128]{1,0:T(8,128)(2,1)S(1)} %add_convert_fusion.2), channel_id=1, replica_groups=mesh['kv'=4,'tp'=8] {'tp'}, dimensions={1}, use_global_device_ids=true | all-gather | bytes 589824 | tf_op jit(solution)/shard_map/all_gather | solution.py:169
  137.1 2.0 convolution_convert_fusion.8
  140.4 2.0 convolution_convert_fusion.7
  142.5 2.4 convolution_convert_fusion.5
  145.1 9.9 %all-reduce = bf16[256]{0:T(256)(128)(2,1)S(1)} all-reduce(bf16[256]{0:T(256)(128)(2,1)S(1)} %fusion.5), channel_id=4, replica_groups=mesh['kv'=4,'tp'=8] {'kv'}, use_global_device_ids=true, to_apply=%region_7.8.clone | all-reduce | flops 256 | bytes 1024
  155.2 2.4 convolution_convert_fusion.6
  157.8 4.2 %reduce-scatter.16.cloned.1.call-done = bf16[64,256]{1,0:T(8,128)(2,1)} async-done(((bf16[256,256]{1,0:T(8,128)(2,1)}), bf16[64,256]{1,0:T(8,128)(2,1)}) %reduce-scatter.16.cloned.1.call-update) | async-done | bytes 32784 | tf_op jit(solution)/shard_map/reduce_scatter | solution.py:71
  162.0 26.8 %reduce-scatter.18.cloned.1.call-done = bf16[64,256]{1,0:T(8,128)(2,1)} async-done(((bf16[256,256]{1,0:T(8,128)(2,1)}), bf16[64,256]{1,0:T(8,128)(2,1)}) %reduce-scatter.18.cloned.1.call-update) | async-done | bytes 32784 | tf_op jit(solution)/shard_map/reduce_scatter | solution.py:74
  190.2 26.1 %reduce-scatter.20.cloned.1.call-done = bf16[64,512]{1,0:T(8,128)(2,1)} async-done(((bf16[256,512]{1,0:T(8,128)(2,1)}), bf16[64,512]{1,0:T(8,128)(2,1)}) %reduce-scatter.20.cloned.1.call-update) | async-done | bytes 65552 | tf_op jit(solution)/shard_map/reduce_scatter | solution.py:77
  217.3 5.3 %multiply_add_fusion = f32[64,4,64,128]{3,2,1,0:T(8,128)S(1)} fusion(f32[64,4,64,128]{3,2,1,0:T(8,128)} %param.18, f32[64,4,128]{2,1,0:T(4,128)S(1)} %mul.290, f32[64,4,64]{2,1,0:T(4,128)S(1)} %copy.21, f32[4]{0:T(128)S(1)} %exponential_subtract_fusion), kind=kLoop, calls=%fused_computation | loop fusion | flops 6291456 | bytes 16973840 | tf_op jit(solution)/shard_map/add | solution.py:99
  222.6 7.3 %fusion.30 = f32[64,4,1,128]{3,2,1,0:T(1,128)S(1)} fusion(f32[64,4,64,1]{2,3,1,0:T(1,128)S(1)} %copy.22, f32[64,4,64,128]{3,2,1,0:T(8,128)S(1)} %multiply_add_fusion), kind=kOutput, calls=%fused_computation.64 | convolution fusion | flops 25165824 | bytes 8585216 | tf_op jit(solution)/shard_map/bhk,bhkv->bhv/dot_general | solution.py:102
  230.6 12.7 %reduce-scatter.14.cloned.1.call-done = bf16[64,512]{1,0:T(8,128)(2,1)} async-done(((bf16[256,512]{1,0:T(8,128)(2,1)}), bf16[64,512]{1,0:T(8,128)(2,1)}) %reduce-scatter.14.cloned.1.call-update) | async-done | bytes 65552 | tf_op jit(solution)/shard_map/reduce_scatter | solution.py:80
  244.3 9.3 %all_gather.14 = bf16[256,512]{1,0:T(8,128)(2,1)S(1)} all-gather(bf16[64,512]{1,0:T(8,128)(2,1)S(1)} %fusion.21), channel_id=1, replica_groups=mesh['kv'=4,'tp'=8] {'kv'}, dimensions={0}, use_global_device_ids=true | all-gather | bytes 327680 | tf_op jit(solution)/shard_map/all_gather | solution.py:110
  253.6 1.7 convolution_convert_fusion.4
  255.2 1.0 copy.26
  256.3 31.4 %reduce-scatter.24.cloned.1.call-done = bf16[128,256]{1,0:T(8,128)(2,1)} async-done(((bf16[1024,256]{1,0:T(8,128)(2,1)}), bf16[128,256]{1,0:T(8,128)(2,1)}) %reduce-scatter.24.cloned.1.call-update) | async-done | bytes 65552
  288.7 14.2 %all_gather.15 = bf16[256,1024]{1,0:T(8,128)(2,1)S(1)} all-gather(bf16[256,128]{1,0:T(8,128)(2,1)S(1)} %add_convert_fusion.1), channel_id=1, replica_groups=mesh['kv'=4,'tp'=8] {'tp'}, dimensions={1}, use_global_device_ids=true | all-gather | bytes 589824 | tf_op jit(solution)/shard_map/all_gather | solution.py:169
  302.8 3.7 convolution_convert_fusion
  306.5 1.9 convolution_convert_fusion.1
  308.6 10.2 %psum.46 = bf16[256]{0:T(256)(128)(2,1)S(1)} all-reduce(bf16[256]{0:T(256)(128)(2,1)S(1)} %fusion.7), channel_id=1, replica_groups=mesh['kv'=4,'tp'=8] {'kv'}, use_global_device_ids=true, to_apply=%region_16.17 | all-reduce | flops 256 | bytes 1024 | tf_op jit(solution)/shard_map/psum | solution.py:45
  318.9 46.7 %all-reduce.6.cloned.1.call-done = (bf16[256,1408]{1,0:T(8,128)(2,1)}, bf16[256,1408]{1,0:T(8,128)(2,1)}) async-done(((bf16[256,1408]{1,0:T(8,128)(2,1)}, bf16[256,1408]{1,0:T(8,128)(2,1)}), (bf16[256,1408]{1,0:T(8,128)(2,1)}, bf16[256,1408]{1,0:T(8,128)(2,1)})) %all-reduce.6.cloned.1.call-update) | async-done | bytes 1441808 | tf_op jit(solution)/shard_map/psum | solution.py:44
  365.6 3.4 fusion.1
  369.0 1.0 copy.28
  370.0 31.6 %reduce-scatter.26.cloned.1.call-done = bf16[128,256]{1,0:T(8,128)(2,1)} async-done(((bf16[1024,256]{1,0:T(8,128)(2,1)}), bf16[128,256]{1,0:T(8,128)(2,1)}) %reduce-scatter.26.cloned.1.call-update) | async-done | bytes 65552
  (69 shorter events, 9.5 us)
Async XLA Ops:
  7.2 15.9 %copy-start = (bf16[1024,1408]{1,0:T(8,128)(2,1)S(1)}, bf16[1024,1408]{1,0:T(8,128)(2,1)}, u32[]{:S(2)}) copy-start(bf16[1024,1408]{1,0:T(8,128)(2,1)} %param.21) | copy-start | bytes 8650756
  7.2 18.4 %copy-start.6 = (f32[1024]{0:T(1024)S(1)}, f32[1024]{0:T(1024)}, u32[]{:S(2)}) copy-start(f32[1024]{0:T(1024)} %param.19) | copy-start | bytes 12292
  7.2 79.0 %all-reduce.8.cloned.1.call-start = ((), (), s32[]{:S(2)}) async-start(), calls=%async_computation.15 | async-start | bytes 2883584 | tf_op jit(solution)/shard_map/psum | solution.py:44
  7.2 18.3 %copy-start.4 = (bf16[1024,1408]{1,0:T(8,128)(2,1)S(1)}, bf16[1024,1408]{1,0:T(8,128)(2,1)}, u32[]{:S(2)}) copy-start(bf16[1024,1408]{1,0:T(8,128)(2,1)} %param.20) | copy-start | bytes 8650756
  27.5 94.6 %reduce-scatter.22.cloned.1.call-start = ((), (), s32[]{:S(2)}) async-start(), calls=%async_computation.11 | async-start | bytes 589824
  86.2 36.8 %copy-start.2 = (bf16[256,128]{1,0:T(8,128)(2,1)S(1)}, bf16[256,128]{1,0:T(8,128)(2,1)}, u32[]{:S(2)}) copy-start(bf16[256,128]{1,0:T(8,128)(2,1)} %param.17) | copy-start | bytes 196612
  86.2 50.9 %copy-start.7 = (f32[1024]{0:T(1024)S(1)}, f32[1024]{0:T(1024)}, u32[]{:S(2)}) copy-start(f32[1024]{0:T(1024)} %param.23) | copy-start | bytes 12292
  89.7 49.5 %copy-start.9 = (u32[32]{0:T(128)S(1)}, u32[32]{0:T(128)}, u32[]{:S(2)}) copy-start(u32[32]{0:T(128)} %constant.53) | copy-start | bytes 388
  90.7 71.3 %reduce-scatter.16.cloned.1.call-start = ((), (), s32[]{:S(2)}) async-start(), calls=%async_computation.8 | async-start | bytes 163840 | tf_op jit(solution)/shard_map/reduce_scatter | solution.py:71
  139.1 49.7 %reduce-scatter.18.cloned.1.call-start = ((), (), s32[]{:S(2)}) async-start(), calls=%async_computation.9 | async-start | bytes 163840 | tf_op jit(solution)/shard_map/reduce_scatter | solution.py:74
  142.4 73.9 %reduce-scatter.20.cloned.1.call-start = ((), (), s32[]{:S(2)}) async-start(), calls=%async_computation.10 | async-start | bytes 327680 | tf_op jit(solution)/shard_map/reduce_scatter | solution.py:77
  144.9 98.4 %reduce-scatter.14.cloned.1.call-start = ((), (), s32[]{:S(2)}) async-start(), calls=%async_computation.7 | async-start | bytes 327680 | tf_op jit(solution)/shard_map/reduce_scatter | solution.py:80
  157.6 130.1 %reduce-scatter.24.cloned.1.call-start = ((), (), s32[]{:S(2)}) async-start(), calls=%async_computation.12 | async-start | bytes 589824
  222.6 7.4 %copy-start.1 = (f32[64,4,64,128]{3,2,1,0:T(8,128)}, f32[64,4,64,128]{3,2,1,0:T(8,128)S(1)}, u32[]{:S(2)}) copy-start(f32[64,4,64,128]{3,2,1,0:T(8,128)S(1)} %multiply_add_fusion) | copy-start | bytes 25165828
  222.6 20.7 %copy-start.3 = (f32[512]{0:T(512)S(1)}, f32[512]{0:T(512)}, u32[]{:S(2)}) copy-start(f32[512]{0:T(512)} %param.28) | copy-start | bytes 6148
  230.0 72.8 %copy-start.8 = (f32[1024]{0:T(1024)S(1)}, f32[1024]{0:T(1024)}, u32[]{:S(2)}) copy-start(f32[1024]{0:T(1024)} %param.30) | copy-start | bytes 12292
  256.2 109.3 %all-reduce.6.cloned.1.call-start = ((), (), s32[]{:S(2)}) async-start(), calls=%async_computation.14 | async-start | bytes 2883584 | tf_op jit(solution)/shard_map/psum | solution.py:44
  288.6 17.9 %copy-start.5 = (bf16[1024,1408]{1,0:T(8,128)(2,1)S(1)}, bf16[1024,1408]{1,0:T(8,128)(2,1)}, u32[]{:S(2)}) copy-start(bf16[1024,1408]{1,0:T(8,128)(2,1)} %param.31) | copy-start | bytes 8650756
  308.4 93.2 %reduce-scatter.26.cloned.1.call-start = ((), (), s32[]{:S(2)}) async-start(), calls=%async_computation.13 | async-start | bytes 589824
Sparse Core Ops, SparseCore 0:
  27.6 58.5 all-reduce.7
  90.8 31.1 reduce-scatter.21
  139.2 22.7 reduce-scatter.15
  164.6 24.1 reduce-scatter.17
  192.0 24.3 reduce-scatter.19
  218.9 24.3 reduce-scatter.13
  256.4 31.2 reduce-scatter.23
  308.5 56.9 all-reduce.5
  370.1 31.3 reduce-scatter.25
where the time goes:
time: 411 us; the launch traced here: 410 us
  waiting for transfers between devices  259 us (63%)
  blocking collectives  83.5 us (20%)
  matrix products  34.6 us (8%)
  between operations  14.8 us (4%)
  other arithmetic  10.2 us (2%)
  local copies, waits for them, and re-layouts  6.92 us (2%)
    psum x2, waiting for transfers between devices, channel_mix(): lax.psum(up_part.astype(jnp.bfloat16), 'kv').astype(jnp.float32)  95.1 us
    unnamed x12, waiting for transfers between devices  94.3 us
    all_gather x2, blocking collectives, shards(): widened = lax.all_gather(own_columns, 'tp', axis=1, tiled=True)  28.2 us
    reduce_scatter x1, waiting for transfers between devices, token_mix(): lax.psum_scatter(key_part.astype(jnp.bfloat16), 'kv', scatter_dimension=0...  26.8 us
    reduce_scatter x1, waiting for transfers between devices, token_mix(): lax.psum_scatter(value_part.astype(jnp.bfloat16), 'kv', scatter_dimension...  26.1 us
    psum x2, blocking collectives, channel_mix(): lax.psum(squares.astype(jnp.bfloat16), 'kv').astype(jnp.float32)  20.3 us
    all_gather x1, blocking collectives, shards(): widened = lax.all_gather(tokens, 'tp', axis=1, tiled=True)  15.8 us
    reduce_scatter x1, waiting for transfers between devices, token_mix(): lax.psum_scatter(gate_part.astype(jnp.bfloat16), 'kv', scatter_dimension=...  12.7 us
  transfers between devices with their start and end apart: 9, of which 9 were waited for; matrix products, arithmetic and copies ran while one was open for 6% of the time, Pallas kernels for 0%

commit v1 on v0

--- a/solution.py
+++ b/solution.py
@@ -1,6 +1,8 @@
 import jax
 import jax.numpy as jnp
 from jax import lax
+from jax.experimental import pallas as pl
+from jax.experimental.pallas import tpu as pltpu
 from jax.sharding import PartitionSpec as P
 
 D = 4096
@@ -170,6 +172,524 @@
     return (own_columns, state_out)
 
 
+MESH = pl.DeviceIdType.MESH
+LANES = 128
+F32 = jnp.float32
+BF16 = jnp.bfloat16
+VMEM_BYTES = 60 * 1024 * 1024
+
+
+def send(src, dst, send_sem, recv_sem, target):
+    copy = pltpu.make_async_remote_copy(
+        src_ref=src,
+        dst_ref=dst,
+        send_sem=send_sem,
+        recv_sem=recv_sem,
+        device_id=target,
+        device_id_type=MESH,
+    )
+    copy.start()
+    return copy
+
+
+class Place:
+    def __init__(self, groups, width):
+        self.groups, self.width, self.chips = groups, width, width // 2
+        self.kv = lax.axis_index("kv")
+        self.tp = lax.axis_index("tp")
+        self.chip = self.tp // 2
+        self.core = lax.rem(self.tp, 2)
+        self.partner = {"tp": 2 * self.chip + 1 - self.core}
+
+    def chip_peer(self, d):
+        return lax.rem(self.chip + d, self.chips)
+
+    def tp_peer(self, d):
+        return {"tp": 2 * self.chip_peer(d) + self.core}
+
+    def tp_origin(self, d):
+        return 2 * lax.rem(self.chip + self.chips - d, self.chips) + self.core
+
+    def kv_index(self, d):
+        return lax.rem(self.kv + d, self.groups)
+
+    def kv_peer(self, d):
+        return {"kv": self.kv_index(d)}
+
+    def barrier(self):
+        barrier = pltpu.get_barrier_semaphore()
+        targets = [self.partner]
+        targets += [self.tp_peer(d) for d in range(1, self.chips)]
+        targets += [self.kv_peer(d) for d in range(1, self.groups)]
+        for target in targets:
+            pl.semaphore_signal(barrier, inc=1, device_id=target, device_id_type=MESH)
+        pl.semaphore_wait(barrier, len(targets))
+
+
+def gather_scratch(place_shape, rows, cols):
+    groups, width = place_shape
+    chips = width // 2
+    sems = [pltpu.SemaphoreType.DMA((chips,))] * 4
+    return [pltpu.VMEM((width, rows, cols), BF16)] + sems
+
+
+def gather_tp(place, own, scratch):
+    blocks, send_far, recv_far, send_near, recv_near = scratch
+    me = place.tp
+    far = [
+        send(own, blocks.at[me], send_far.at[d], recv_far.at[d], place.tp_peer(d))
+        for d in range(1, place.chips)
+    ]
+    near = [send(own, blocks.at[me], send_near.at[0], recv_near.at[0], place.partner)]
+    blocks[me] = own[...]
+    for d in range(1, place.chips):
+        far[d - 1].wait_recv()
+        block = blocks.at[place.tp_origin(d)]
+        near.append(send(block, block, send_near.at[d], recv_near.at[d], place.partner))
+    for copy in near:
+        copy.wait_recv()
+    for copy in far + near:
+        copy.wait_send()
+    return blocks
+
+
+def scale_scratch(place_shape, rows, cols):
+    groups, width = place_shape
+    sems = [pltpu.SemaphoreType.DMA((groups,))] * 2
+    return [
+        pltpu.VMEM((rows, width * cols), BF16),
+        pltpu.VMEM((groups, rows // groups, LANES), BF16),
+        pltpu.VMEM((groups, rows // groups, LANES), BF16),
+    ] + sems
+
+
+def scale(place, blocks, gain, scratch):
+    scaled, sq_out, sq_in, send_sem, recv_sem = scratch
+    width, rows, cols = blocks.shape
+    part = rows // place.groups
+    total = jnp.zeros((rows, 1), F32)
+    for t in range(width):
+        block = blocks[t].astype(F32)
+        at = slice(t * cols, (t + 1) * cols)
+        scaled[:, at] = (block * gain[:, at]).astype(BF16)
+        total = total + jnp.sum(block * block, axis=1, keepdims=True)
+    high = total.astype(BF16).astype(F32)
+    low = total - high
+    lane = lax.broadcasted_iota(jnp.int32, (rows, LANES), 1)
+    both = jnp.where(lane < LANES // 2, high, low).astype(BF16)
+    for k in range(place.groups):
+        sq_out[k] = both[k * part : (k + 1) * part]
+    copies = [
+        send(
+            sq_out.at[place.kv_index(d)],
+            sq_in.at[d],
+            send_sem.at[d],
+            recv_sem.at[d],
+            place.kv_peer(d),
+        )
+        for d in range(1, place.groups)
+    ]
+
+    def inverse_rms():
+        for copy in copies:
+            copy.wait()
+        both = sq_out[place.kv].astype(F32)
+        for d in range(1, place.groups):
+            both = both + sq_in[d].astype(F32)
+        summed = jnp.sum(both, axis=1, keepdims=True) / (LANES // 2)
+        return lax.rsqrt(summed / D + EPS_RMS)
+
+    return scaled, inverse_rms
+
+
+def spans(count, pieces):
+    cuts = [count * i // pieces for i in range(pieces + 1)]
+    return [(a, b) for a, b in zip(cuts, cuts[1:]) if b > a]
+
+
+FF_PIECES = 3
+
+
+def hidden_scratch(place_shape, rows, units):
+    groups, width = place_shape
+    part, tiles = rows // groups, units // LANES
+    exchange = pltpu.VMEM((groups, tiles, 2, part, LANES), BF16)
+    sems = [pltpu.SemaphoreType.DMA((FF_PIECES, groups))] * 4
+    return [exchange, exchange, pltpu.VMEM((rows, units), BF16)] + sems
+
+
+def hidden_units(place, scaled, inverse_rms, w_gate, w_up, scratch):
+    out, into, hidden, send_part, recv_part, send_hid, recv_hid = scratch
+    rows, units = hidden.shape
+    groups = place.groups
+    part, tiles = rows // groups, units // LANES
+    pieces = spans(tiles, FF_PIECES)
+    own_rows = pl.ds(pl.multiple_of(place.kv * part, part), part)
+
+    def lanes(j):
+        return pl.ds(pl.multiple_of(j * LANES, LANES), LANES)
+
+    def products(j, carry):
+        weights = jnp.concatenate([w_gate[:, lanes(j)], w_up[:, lanes(j)]], axis=1)
+        result = jnp.dot(scaled[...], weights, preferred_element_type=F32).astype(BF16)
+        for k in range(groups):
+            for side in range(2):
+                out[k, j, side] = result[
+                    k * part : (k + 1) * part, side * LANES : (side + 1) * LANES
+                ]
+        return carry
+
+    part_copies = []
+    for p, (low, high) in enumerate(pieces):
+        lax.fori_loop(low, high, products, 0)
+        span = pl.ds(low, high - low)
+        part_copies.append(
+            [
+                send(
+                    out.at[place.kv_index(d), span],
+                    into.at[d, span],
+                    send_part.at[p, d],
+                    recv_part.at[p, d],
+                    place.kv_peer(d),
+                )
+                for d in range(1, groups)
+            ]
+        )
+    factor = inverse_rms()
+
+    def activation(j, carry):
+        sums = []
+        for side in range(2):
+            total = out[place.kv, j, side].astype(F32)
+            for d in range(1, groups):
+                total = total + into[d, j, side].astype(F32)
+            sums.append(total * factor)
+        value = sums[0] / (1.0 + jnp.exp(-sums[0])) * sums[1]
+        hidden[own_rows, lanes(j)] = value.astype(BF16)
+        return carry
+
+    hid_copies = []
+    for p, (low, high) in enumerate(pieces):
+        for copy in part_copies[p]:
+            copy.wait_recv()
+        lax.fori_loop(low, high, activation, 0)
+        block = hidden.at[own_rows, pl.ds(low * LANES, (high - low) * LANES)]
+        hid_copies += [
+            send(block, block, send_hid.at[p, d], recv_hid.at[p, d], place.kv_peer(d))
+            for d in range(1, groups)
+        ]
+    for copies in part_copies:
+        for copy in copies:
+            copy.wait_send()
+    for copy in hid_copies:
+        copy.wait()
+    return hidden
+
+
+def branch_scratch(place_shape, rows, cols):
+    groups, width = place_shape
+    chips = width // 2
+    half = (chips, rows, cols)
+    sems = [pltpu.SemaphoreType.DMA((chips,))] * 2
+    near = [pltpu.SemaphoreType.DMA] * 2
+    return [
+        pltpu.VMEM(half, BF16),
+        pltpu.VMEM(half, BF16),
+        pltpu.VMEM(half, F32),
+        pltpu.VMEM(half, BF16),
+        pltpu.VMEM(half, BF16),
+    ] + near + sems
+
+
+def branch(place, left, weight, factor, scratch):
+    away, near_in, own, pair, far_in, send_near, recv_near, send_far, recv_far = scratch
+    chips, rows, cols = away.shape
+
+    def products(core, into):
+        def step(i, carry):
+            columns = [
+                weight[:, pl.ds(pl.multiple_of((2 * (2 * i + s) + core) * cols, cols), cols)]
+                for s in range(2)
+            ]
+            result = factor * jnp.dot(
+                left[...], jnp.concatenate(columns, axis=1), preferred_element_type=F32
+            )
+            for s in range(2):
+                into[2 * i + s] = result[:, s * cols : (s + 1) * cols].astype(into.dtype)
+            return carry
+
+        lax.fori_loop(0, chips // 2, step, 0)
+
+    products(1 - place.core, away)
+    near = send(away, near_in, send_near, recv_near, place.partner)
+    products(place.core, own)
+    near.wait()
+    far = []
+    for d in range(1, chips):
+        chip = place.chip_peer(d)
+        pair[chip] = (own[chip] + near_in[chip].astype(F32)).astype(BF16)
+        far.append(
+            send(pair.at[chip], far_in.at[d], send_far.at[d], recv_far.at[d], place.tp_peer(d))
+        )
+    total = own[place.chip] + near_in[place.chip].astype(F32)
+    for copy in far:
+        copy.wait()
+    for d in range(1, chips):
+        total = total + far_in[d].astype(F32)
+    return total
+
+
+def project_scratch(place_shape, rows, steps):
+    groups, width = place_shape
+    exchange = pltpu.VMEM((groups, steps, rows // groups, 2 * LANES), BF16)
+    sems = [pltpu.SemaphoreType.DMA((4, groups))] * 2
+    return [exchange, exchange] + sems
+
+
+def project(place, scaled, inverse_rms, weights, result_ref, scratch):
+    out, into, send_sem, recv_sem = scratch
+    groups, steps, part, wide = out.shape
+    base, copies, where = 0, [], []
+    for p, weight in enumerate(weights):
+        count = weight.shape[1] // wide
+
+        def products(j, carry, weight=weight, base=base):
+            at = pl.ds(pl.multiple_of(j * wide, wide), wide)
+            result = jnp.dot(scaled[...], weight[:, at], preferred_element_type=F32).astype(BF16)
+            for k in range(groups):
+                out[k, base + j] = result[k * part : (k + 1) * part]
+            return carry
+
+        lax.fori_loop(0, count, products, 0)
+        span = pl.ds(base, count)
+        copies.append(
+            [
+                send(
+                    out.at[place.kv_index(d), span],
+                    into.at[d, span],
+                    send_sem.at[p, d],
+                    recv_sem.at[p, d],
+                    place.kv_peer(d),
+                )
+                for d in range(1, groups)
+            ]
+        )
+        where.append((base, base + count))
+        base += count
+    factor = inverse_rms()
+    for p, (low, high) in enumerate(where):
+        for copy in copies[p]:
+            copy.wait_recv()
+        for j in range(low, high):
+            total = out[place.kv, j].astype(F32)
+            for d in range(1, groups):
+                total = total + into[d, j].astype(F32)
+            result_ref[:, j * wide : (j + 1) * wide] = total * factor
+    for group in copies:
+        for copy in group:
+            copy.wait_send()
+
+
+def take(refs, count):
+    return [refs.pop(0) for _ in range(count)]
+
+
+def load_all(sources, buffers, sem):
+    copies = [
+        pltpu.make_async_copy(source, buffer, sem.at[i])
+        for i, (source, buffer) in enumerate(zip(sources, buffers))
+    ]
+    for copy in copies:
+        copy.start()
+    return copies
+
+
+def first_kernel(shape, *refs):
+    refs = list(refs)
+    tokens, gain, mix_gain = take(refs, 3)
+    sources = take(refs, 7)
+    own_out, mix_out = take(refs, 2)
+    buffers = take(refs, 7)
+    (load_sem, own) = take(refs, 2)
+    gather_a, gather_b = take(refs, 5), take(refs, 5)
+    scale_a, scale_b = take(refs, 5), take(refs, 5)
+    hidden_s, branch_s, project_s = take(refs, 7), take(refs, 9), take(refs, 4)
+    place = Place(*shape)
+    loads = load_all(sources, buffers, load_sem)
+    w_gate, w_up, w_down = buffers[:3]
+    place.barrier()
+    blocks = gather_tp(place, tokens, gather_a)
+    scaled, inverse_rms = scale(place, blocks, gain, scale_a)
+    loads[0].wait()
+    loads[1].wait()
+    hidden = hidden_units(place, scaled, inverse_rms, w_gate, w_up, hidden_s)
+    loads[2].wait()
+    total = branch(place, hidden, w_down, 0.5, branch_s)
+    own[...] = (tokens[...].astype(F32) + total).astype(BF16)
+    own_out[...] = own[...]
+    blocks = gather_tp(place, own, gather_b)
+    scaled, inverse_rms = scale(place, blocks, mix_gain, scale_b)
+    for load in loads[3:]:
+        load.wait()
+    project(place, scaled, inverse_rms, buffers[3:], mix_out, project_s)
+
+
+def last_kernel(shape, *refs):
+    refs = list(refs)
+    heads, resid, gain = take(refs, 3)
+    sources = take(refs, 4)
+    (result,) = take(refs, 1)
+    buffers = take(refs, 4)
+    load_sem, own, joined, send_heads, recv_heads = take(refs, 5)
+    gather_a, scale_a = take(refs, 5), take(refs, 5)
+    hidden_s, branch_a, branch_b = take(refs, 7), take(refs, 9), take(refs, 9)
+    place = Place(*shape)
+    loads = load_all(sources, buffers, load_sem)
+    w_out, w_gate, w_up, w_down = buffers
+    place.barrier()
+    part = heads.shape[0]
+    rows = joined.at[pl.ds(pl.multiple_of(place.kv * part, part), part)]
+    copies = [
+        send(heads, rows, send_heads.at[d], recv_heads.at[d], place.kv_peer(d))
+        for d in range(1, place.groups)
+    ]
+    rows[...] = heads[...]
+    for copy in copies:
+        copy.wait()
+    loads[0].wait()
+    total = branch(place, joined, w_out, 1.0, branch_a)
+    own[...] = (resid[...].astype(F32) + total).astype(BF16)
+    blocks = gather_tp(place, own, gather_a)
+    scaled, inverse_rms = scale(place, blocks, gain, scale_a)
+    loads[1].wait()
+    loads[2].wait()
+    hidden = hidden_units(place, scaled, inverse_rms, w_gate, w_up, hidden_s)
+    loads[3].wait()
+    total = branch(place, hidden, w_down, 0.5, branch_b)
+    result[...] = (own[...].astype(F32) + total).astype(BF16)
+
+
+def call(kernel, shape, small, large, outs, scratch, collective):
+    vmem = pl.BlockSpec(memory_space=pltpu.VMEM)
+    hbm = pl.BlockSpec(memory_space=pl.ANY)
+    buffers = [pltpu.VMEM(w.shape, w.dtype) for w in large]
+    return pl.pallas_call(
+        lambda *refs: kernel(shape, *refs),
+        name=kernel.__name__,
+        out_shape=outs,
+        in_specs=[vmem] * len(small) + [hbm] * len(large),
+        out_specs=jax.tree.map(lambda _: vmem, outs),
+        scratch_shapes=buffers + [pltpu.SemaphoreType.DMA((len(large),))] + scratch,
+        compiler_params=pltpu.CompilerParams(
+            collective_id=collective, has_side_effects=True, vmem_limit_bytes=VMEM_BYTES
+        ),
+    )(*small, *large)
+
+
+def retain(mix, past_state, head_gain, key_cols, value_cols):
+    row_count, local_heads = past_state.shape[:2]
+    queries = mix[:, :key_cols]
+    keys_now = mix[:, key_cols : 2 * key_cols]
+    values_now = mix[:, 2 * key_cols : 2 * key_cols + value_cols]
+    gate_now = mix[:, 2 * key_cols + value_cols :]
+    queries = rotate(queries.reshape(row_count, local_heads, HEAD_K)) * HEAD_K ** (-0.5)
+    keys_now = rotate(keys_now.reshape(row_count, local_heads, HEAD_K))
+    values_now = values_now.reshape(row_count, local_heads, HEAD_V)
+    head_level = (lax.axis_index("tp") * local_heads + jnp.arange(local_heads)).astype(F32)
+    retained = 1.0 - jnp.exp2(-5.0 - 16.0 * head_level / (HEADS - 1))
+    new_state = (
+        retained[None, :, None, None] * past_state
+        + keys_now[:, :, :, None] * values_now[:, :, None, :]
+    )
+    retrieved = jnp.einsum("bhk,bhkv->bhv", queries, new_state, precision=lax.Precision.HIGHEST)
+    head_mean = jnp.mean(retrieved, axis=-1, keepdims=True)
+    variance = jnp.mean(jnp.square(retrieved - head_mean), axis=-1, keepdims=True)
+    normed = ((retrieved - head_mean) * lax.rsqrt(variance + EPS_GROUP)).reshape(
+        row_count, local_heads * HEAD_V
+    )
+    return (jax.nn.silu(gate_now) * (normed * head_gain)).astype(BF16), new_state
+
+
+def fused_shards(
+    tokens,
+    past_state,
+    first_gain,
+    first_gate,
+    first_up,
+    first_down,
+    mix_gain,
+    query_weight,
+    key_weight,
+    value_weight,
+    output_gate_weight,
+    head_gain,
+    out_weight,
+    second_gain,
+    second_gate,
+    second_up,
+    second_down,
+):
+    shape = (lax.axis_size("kv"), lax.axis_size("tp"))
+    rows, cols = tokens.shape
+    part, units = rows // shape[0], first_gate.shape[1]
+    mix_weights = (query_weight, key_weight, value_weight, output_gate_weight)
+    mix_cols = sum(w.shape[1] for w in mix_weights)
+    gather, scaling = gather_scratch(shape, rows, cols), scale_scratch(shape, rows, cols)
+    hidden, branches = hidden_scratch(shape, rows, units), branch_scratch(shape, rows, cols)
+    own = [pltpu.VMEM((rows, cols), BF16)]
+    first, mix = call(
+        first_kernel,
+        shape,
+        (tokens, first_gain[None], mix_gain[None]),
+        (first_gate, first_up, first_down) + mix_weights,
+        (
+            jax.ShapeDtypeStruct((rows, cols), BF16),
+            jax.ShapeDtypeStruct((part, mix_cols), F32),
+        ),
+        own
+        + gather * 2
+        + scaling * 2
+        + hidden
+        + branches
+        + project_scratch(shape, rows, mix_cols // (2 * LANES)),
+        0,
+    )
+    heads, new_state = retain(
+        mix, past_state, head_gain, query_weight.shape[1], value_weight.shape[1]
+    )
+    mixed = call(
+        last_kernel,
+        shape,
+        (heads, first, second_gain[None]),
+        (out_weight, second_gate, second_up, second_down),
+        jax.ShapeDtypeStruct((rows, cols), BF16),
+        own
+        + [pltpu.VMEM((rows, heads.shape[1]), BF16)]
+        + [pltpu.SemaphoreType.DMA((shape[0],))] * 2
+        + gather
+        + scaling
+        + hidden
+        + branches * 2,
+        1,
+    )
+    return mixed, new_state
+
+
+def layer(*arrays):
+    groups, width = lax.axis_size("kv"), lax.axis_size("tp")
+    tokens, first_gate, mix_weights = arrays[0], arrays[3], arrays[7:11]
+    rows, cols = tokens.shape
+    whole_tiles = (
+        groups > 1
+        and width % 4 == 0
+        and cols % LANES == 0
+        and rows % (16 * groups) == 0
+        and first_gate.shape[1] % LANES == 0
+        and all(weight.shape[1] % (2 * LANES) == 0 for weight in mix_weights)
+    )
+    return fused_shards(*arrays) if whole_tiles else shards(*arrays)
+
+
 def solution(mesh):
     in_specs = (
         P(None, ("kv", "tp")),
@@ -191,4 +711,4 @@
         P("tp", "kv"),
     )
     out_specs = (P(None, ("kv", "tp")), P("kv", "tp", None, None))
-    return jax.shard_map(shards, mesh=mesh, in_specs=in_specs, out_specs=out_specs, check_vma=False)
+    return jax.shard_map(layer, mesh=mesh, in_specs=in_specs, out_specs=out_specs, check_vma=False)

time: 411 us -> 158 us (0.38)
  waiting for transfers between devices: 259 us -> 0 us
  Pallas kernels: 0 us -> 135 us
  blocking collectives: 83.5 us -> 0 us
  matrix products: 34.6 us -> 7.33 us
  between operations: 14.8 us -> 0.78 us
    pallas_call x0 -> x2, Pallas kernels: none -> 135 us  [call(): pl.pallas_call(lambda *refs: kernel(shape, *refs), name=kernel.__name__,...]
    psum x2 -> x0, waiting for transfers between devices: 95.1 us -> none  [channel_mix(): lax.psum(up_part.astype(jnp.bfloat16), 'kv').astype(jnp.float32)]
    unnamed x12 -> x0, waiting for transfers between devices: 94.3 us -> none
    reduce_scatter x4 -> x0, waiting for transfers between devices: 69.8 us -> none  [the longest x1 26.8 us: token_mix(): lax.psum_scatter(key_part.astype(jnp.bfloat16), 'kv', scatter_dimension=0...]
    all_gather x4 -> x0, blocking collectives: 53.3 us -> none  [the longest x2 28.2 us: shards(): widened = lax.all_gather(own_columns, 'tp', axis=1, tiled=True)]
    dot_general x12 -> x1, matrix products: 34.6 us -> 7.33 us  [retain(): jnp.einsum('bhk,bhkv->bhv', queries, new_state, precision=lax.Precision.H...]
    psum x2 -> x0, blocking collectives: 20.3 us -> none  [channel_mix(): lax.psum(squares.astype(jnp.bfloat16), 'kv').astype(jnp.float32)]
    unnamed x1 -> x0, blocking collectives: 9.95 us -> none
  transfers between devices with their start and end apart: 9 -> 0, of which waited for: 9 -> 0; matrix products, arithmetic and copies ran while one was open for 6% -> 0% of each run, Pallas kernels for 0% -> 0%
where the time goes in v1:
time: 158 us; the launch traced here: 157 us
  Pallas kernels  135 us (85%)
  other arithmetic  7.67 us (5%)
  matrix products  7.33 us (5%)
  local copies, waits for them, and re-layouts  7.11 us (4%)
    pallas_call x2, Pallas kernels, call(): pl.pallas_call(lambda *refs: kernel(shape, *refs), name=kernel.__name__,...  135 us
    dot_general x1, matrix products, retain(): jnp.einsum('bhk,bhkv->bhv', queries, new_state, precision=lax.Precision.H...  7.33 us
    add x1, other arithmetic, retain(): retained[None, :, None, None] * past_state  5.31 us
    unnamed x5, local copies, waits for them, and re-layouts  4.87 us

profile of v1, /device:TPU:0, one launch (start us, length us, event | category | flops | bytes accessed | tf_op | source)
XLA Modules:
  0.0 157.5 jit_solution(9398572196782290367)
XLA Ops:
  0.7 72.3 %first_kernel.1 = (bf16[256,128]{1,0:T(8,128)(2,1)}, f32[64,1536]{1,0:T(8,128)}) custom-call(bf16[256,128]{1,0:T(8,128)(2,1)} %refs_0_.1, f32[1,1024]{1,0:T(1,128)} %bitcast.24, f32[1,1024]{1,0:T(1,128)} %bitcast.25, bf16[1024,1408]{1,0:T(8,128)(2,1)} %refs_3_.2, bf16[1024,1408]{1,0:T(8,128)(2,1)} %refs_4_.2, bf16[1408,1024]{1,0:T(8,128)(2,1)} %refs_5_.2, ...), custom_call_target="tpu_custom_call" | custom-call | tf_op jit(solution)/shard_map/first_kernel/pallas_call | solution.py:576
  73.0 0.9 slice.31
  74.0 0.9 fusion.5
  74.9 0.1 copy.27
  75.0 0.1 copy.26
  75.1 0.1 multiply_subtract_fusion
  75.2 0.1 copy.23
  75.3 0.1 copy.24
  75.5 5.3 %multiply_add_fusion = f32[64,4,64,128]{3,2,1,0:T(8,128)S(1)} fusion(f32[64,4,64,128]{3,2,1,0:T(8,128)} %param.18, f32[64,4,128]{2,1,0:T(4,128)S(1)} %mul.164, f32[64,4,64]{2,1,0:T(4,128)S(1)} %copy.23, f32[4]{0:T(128)S(1)} %exponential_subtract_fusion), kind=kLoop, calls=%fused_computation | loop fusion | flops 6291456 | bytes 16973840 | tf_op jit(solution)/shard_map/add | solution.py:601
  80.8 0.0 copy-start
  80.8 3.4 %copy-done = f32[64,4,64,128]{3,2,1,0:T(8,128)} copy-done((f32[64,4,64,128]{3,2,1,0:T(8,128)}, f32[64,4,64,128]{3,2,1,0:T(8,128)S(1)}, u32[]{:S(2)}) %copy-start) | copy-done | bytes 8388632
  84.2 0.0 copy-start.1
  84.2 7.3 %fusion.6 = f32[64,4,1,128]{3,2,1,0:T(1,128)S(1)} fusion(f32[64,4,64,1]{2,3,1,0:T(1,128)S(1)} %copy.24, f32[64,4,64,128]{3,2,1,0:T(8,128)S(1)} %multiply_add_fusion), kind=kOutput, calls=%fused_computation.20 | convolution fusion | flops 25165824 | bytes 8585216 | tf_op jit(solution)/shard_map/bhk,bhkv->bhv/dot_general | solution.py:604
  91.5 0.1 reduce_sum.18
  91.7 0.2 multiply_reduce_fusion
  91.9 0.2 subtract_multiply_fusion
  92.1 0.0 copy-done.1
  92.1 1.6 %fusion.1.refs_0_ = bf16[64,512]{1,0:T(8,128)(2,1)} fusion(f32[8,8,4,128]{3,2,1,0:T(4,128)S(1)} %bitcast.21, f32[64,1536]{1,0:T(8,128)} %get-tuple-element.4, f32[512]{0:T(512)S(1)} %copy-done.1), kind=kLoop, calls=%fused_computation.3 | loop fusion | flops 229376 | bytes 329728 | tf_op jit(solution)/shard_map/convert_element_type | solution.py:610
  93.7 62.3 %last_kernel.1 = bf16[256,128]{1,0:T(8,128)(2,1)} custom-call(bf16[64,512]{1,0:T(8,128)(2,1)} %fusion.1.refs_0_, bf16[256,128]{1,0:T(8,128)(2,1)} %get-tuple-element.5.refs_1_, f32[1,1024]{1,0:T(1,128)} %bitcast.26, bf16[512,1024]{1,0:T(8,128)(2,1)} %refs_3_.3, bf16[1024,1408]{1,0:T(8,128)(2,1)} %refs_4_.3, bf16[1024,1408]{1,0:T(8,128)(2,1)} %refs_5_.3, ...), custom_call_target="tpu_custom_call" | custom-call | tf_op jit(solution)/shard_map/last_kernel/pallas_call | solution.py:576
  156.0 1.5 copy.31
  (7 shorter events, 0.2 us)
Async XLA Ops:
  80.8 3.4 %copy-start = (f32[64,4,64,128]{3,2,1,0:T(8,128)}, f32[64,4,64,128]{3,2,1,0:T(8,128)S(1)}, u32[]{:S(2)}) copy-start(f32[64,4,64,128]{3,2,1,0:T(8,128)S(1)} %multiply_add_fusion) | copy-start | bytes 25165828
  84.2 8.0 %copy-start.1 = (f32[512]{0:T(512)S(1)}, f32[512]{0:T(512)}, u32[]{:S(2)}) copy-start(f32[512]{0:T(512)} %param.28) | copy-start | bytes 6148

commit v2 on v1

--- a/solution.py
+++ b/solution.py
@@ -176,7 +176,8 @@
 LANES = 128
 F32 = jnp.float32
 BF16 = jnp.bfloat16
-VMEM_BYTES = 60 * 1024 * 1024
+MIB = 1024 * 1024
+FIRST_MIB, STATE_MIB, LAST_MIB = 54, 16, 54
 
 
 def send(src, dst, send_sem, recv_sem, target):
@@ -313,76 +314,131 @@
 def hidden_scratch(place_shape, rows, units):
     groups, width = place_shape
     part, tiles = rows // groups, units // LANES
-    exchange = pltpu.VMEM((groups, tiles, 2, part, LANES), BF16)
-    sems = [pltpu.SemaphoreType.DMA((FF_PIECES, groups))] * 4
-    return [exchange, exchange, pltpu.VMEM((rows, units), BF16)] + sems
+    pair = pltpu.VMEM((2, 2, tiles, part, LANES), BF16)
+    single = pltpu.VMEM((2, tiles, part, LANES), BF16)
+    sems = [pltpu.SemaphoreType.DMA((FF_PIECES, 2, 3))] * 2
+    sems += [pltpu.SemaphoreType.DMA((FF_PIECES, 4))] * 2
+    everything = pltpu.VMEM((2, groups, tiles, part, LANES), BF16)
+    return [everything, pair, single, single, pltpu.VMEM((rows, units), BF16)] + sems
 
 
 def hidden_units(place, scaled, inverse_rms, w_gate, w_up, scratch):
-    out, into, hidden, send_part, recv_part, send_hid, recv_hid = scratch
+    out, into, sums, last, hidden, send_part, recv_part, send_hid, recv_hid = scratch
     rows, units = hidden.shape
     groups = place.groups
     part, tiles = rows // groups, units // LANES
     pieces = spans(tiles, FF_PIECES)
-    own_rows = pl.ds(pl.multiple_of(place.kv * part, part), part)
+    far_y, far_x = place.kv // 2, lax.rem(place.kv, 2)
+    along_x = 2 * far_y + 1 - far_x
+    along_y = 2 * (1 - far_y) + far_x
+    diagonal = 3 - place.kv
+    turns = ((along_x, along_y), (along_y, along_x))
 
     def lanes(j):
         return pl.ds(pl.multiple_of(j * LANES, LANES), LANES)
+
+    def rows_of(k):
+        return pl.ds(pl.multiple_of(k * part, part), part)
 
     def products(j, carry):
         weights = jnp.concatenate([w_gate[:, lanes(j)], w_up[:, lanes(j)]], axis=1)
         result = jnp.dot(scaled[...], weights, preferred_element_type=F32).astype(BF16)
         for k in range(groups):
             for side in range(2):
-                out[k, j, side] = result[
+                out[side, k, j] = result[
                     k * part : (k + 1) * part, side * LANES : (side + 1) * LANES
                 ]
         return carry
 
-    part_copies = []
+    passing, direct, summed, shared, passed = {}, {}, {}, {}, {}
     for p, (low, high) in enumerate(pieces):
         lax.fori_loop(low, high, products, 0)
         span = pl.ds(low, high - low)
-        part_copies.append(
-            [
-                send(
-                    out.at[place.kv_index(d), span],
-                    into.at[d, span],
-                    send_part.at[p, d],
-                    recv_part.at[p, d],
-                    place.kv_peer(d),
+        for side in range(2):
+            near = turns[side][0]
+            for which, block, store in ((1, diagonal, passing), (0, near, direct)):
+                store[p, side] = send(
+                    out.at[side, block, span],
+                    into.at[side, which, span],
+                    send_part.at[p, side, which],
+                    recv_part.at[p, side, which],
+                    {"kv": near},
                 )
-                for d in range(1, groups)
+
+    def pass_on(p):
+        low, high = pieces[p]
+        span = pl.ds(low, high - low)
+        for side in range(2):
+            next_one = turns[side][1]
+            passing[p, side].wait_recv()
+
+            def add(j, carry, side=side, next_one=next_one):
+                total = out[side, next_one, j].astype(F32) + into[side, 1, j].astype(F32)
+                sums[side, j] = total.astype(BF16)
+                return carry
+
+            lax.fori_loop(low, high, add, 0)
+            summed[p, side] = send(
+                sums.at[side, span],
+                last.at[side, span],
+                send_part.at[p, side, 2],
+                recv_part.at[p, side, 2],
+                {"kv": next_one},
+            )
+
+    def activate_piece(p, factor):
+        low, high = pieces[p]
+        for side in range(2):
+            direct[p, side].wait_recv()
+            summed[p, side].wait_recv()
+
+        def activation(j, carry):
+            both = [
+                factor
+                * (
+                    out[side, place.kv, j].astype(F32)
+                    + into[side, 0, j].astype(F32)
+                    + last[side, j].astype(F32)
+                )
+                for side in range(2)
             ]
-        )
+            value = both[0] / (1.0 + jnp.exp(-both[0])) * both[1]
+            hidden[rows_of(place.kv), lanes(j)] = value.astype(BF16)
+            return carry
+
+        lax.fori_loop(low, high, activation, 0)
+        block = hidden.at[rows_of(place.kv), low * LANES : high * LANES]
+        for i, target in enumerate((along_x, along_y)):
+            shared[p, i] = send(
+                block, block, send_hid.at[p, i], recv_hid.at[p, i], {"kv": target}
+            )
+
+    def relay(p):
+        low, high = pieces[p]
+        middle = (low + high) // 2
+        halves = ((low, middle), (middle, high))
+        for i, (origin, target) in enumerate(turns):
+            shared[p, i].wait_recv()
+            start, end = halves[i]
+            block = hidden.at[rows_of(origin), start * LANES : end * LANES]
+            passed[p, i] = send(
+                block, block, send_hid.at[p, 2 + i], recv_hid.at[p, 2 + i], {"kv": target}
+            )
+
     factor = inverse_rms()
-
-    def activation(j, carry):
-        sums = []
-        for side in range(2):
-            total = out[place.kv, j, side].astype(F32)
-            for d in range(1, groups):
-                total = total + into[d, j, side].astype(F32)
-            sums.append(total * factor)
-        value = sums[0] / (1.0 + jnp.exp(-sums[0])) * sums[1]
-        hidden[own_rows, lanes(j)] = value.astype(BF16)
-        return carry
-
-    hid_copies = []
-    for p, (low, high) in enumerate(pieces):
-        for copy in part_copies[p]:
-            copy.wait_recv()
-        lax.fori_loop(low, high, activation, 0)
-        block = hidden.at[own_rows, pl.ds(low * LANES, (high - low) * LANES)]
-        hid_copies += [
-            send(block, block, send_hid.at[p, d], recv_hid.at[p, d], place.kv_peer(d))
-            for d in range(1, groups)
-        ]
-    for copies in part_copies:
-        for copy in copies:
+    count = len(pieces)
+    for stage in range(count + 2):
+        if stage < count:
+            pass_on(stage)
+        if 0 <= stage - 1 < count:
+            activate_piece(stage - 1, factor)
+        if 0 <= stage - 2:
+            relay(stage - 2)
+    for copy in passed.values():
+        copy.wait()
+    for group in (passing, direct, summed, shared):
+        for copy in group.values():
             copy.wait_send()
-    for copy in hid_copies:
-        copy.wait()
     return hidden
 
 
@@ -513,7 +569,7 @@
     (load_sem, own) = take(refs, 2)
     gather_a, gather_b = take(refs, 5), take(refs, 5)
     scale_a, scale_b = take(refs, 5), take(refs, 5)
-    hidden_s, branch_s, project_s = take(refs, 7), take(refs, 9), take(refs, 4)
+    hidden_s, branch_s, project_s = take(refs, 9), take(refs, 9), take(refs, 4)
     place = Place(*shape)
     loads = load_all(sources, buffers, load_sem)
     w_gate, w_up, w_down = buffers[:3]
@@ -542,7 +598,7 @@
     buffers = take(refs, 4)
     load_sem, own, joined, send_heads, recv_heads = take(refs, 5)
     gather_a, scale_a = take(refs, 5), take(refs, 5)
-    hidden_s, branch_a, branch_b = take(refs, 7), take(refs, 9), take(refs, 9)
+    hidden_s, branch_a, branch_b = take(refs, 9), take(refs, 9), take(refs, 9)
     place = Place(*shape)
     loads = load_all(sources, buffers, load_sem)
     w_out, w_gate, w_up, w_down = buffers
@@ -569,9 +625,9 @@
     result[...] = (own[...].astype(F32) + total).astype(BF16)
 
 
-def call(kernel, shape, small, large, outs, scratch, collective):
+def call(kernel, shape, small, large, outs, scratch, collective, limit):
     vmem = pl.BlockSpec(memory_space=pltpu.VMEM)
-    hbm = pl.BlockSpec(memory_space=pl.ANY)
+    hbm = pl.BlockSpec(memory_space=pltpu.HBM)
     buffers = [pltpu.VMEM(w.shape, w.dtype) for w in large]
     return pl.pallas_call(
         lambda *refs: kernel(shape, *refs),
@@ -580,34 +636,91 @@
         in_specs=[vmem] * len(small) + [hbm] * len(large),
         out_specs=jax.tree.map(lambda _: vmem, outs),
         scratch_shapes=buffers + [pltpu.SemaphoreType.DMA((len(large),))] + scratch,
+        cost_estimate=pl.CostEstimate(
+            flops=60_000_000_000, bytes_accessed=100_000_000, transcendentals=0
+        ),
         compiler_params=pltpu.CompilerParams(
-            collective_id=collective, has_side_effects=True, vmem_limit_bytes=VMEM_BYTES
+            collective_id=collective, has_side_effects=True, vmem_limit_bytes=limit * MIB
         ),
     )(*small, *large)
 
 
-def retain(mix, past_state, head_gain, key_cols, value_cols):
+def turned(vectors, cosine, sine):
+    width = vectors.shape[1]
+    half = HEAD_K // 2
+    lane = lax.broadcasted_iota(jnp.int32, vectors.shape, 1)
+    lower = lax.rem(lane, HEAD_K) < half
+    other = jnp.where(
+        lower, pltpu.roll(vectors, width - half, 1), pltpu.roll(vectors, half, 1)
+    )
+    return vectors * cosine + other * sine
+
+
+def retain_kernel(mix, past, cosine, sine, retained, head_gain, heads, new_state, retrieved):
+    count, local_heads = past.shape[:2]
+    key_cols, value_cols = local_heads * HEAD_K, local_heads * HEAD_V
+    queries = turned(mix[:, :key_cols], cosine[...], sine[...]) * HEAD_K ** (-0.5)
+    keys_now = turned(mix[:, key_cols : 2 * key_cols], cosine[...], sine[...])
+    queries, keys_now = queries.T, keys_now.T
+    for b in range(count):
+        for h in range(local_heads):
+            entries = slice(h * HEAD_K, (h + 1) * HEAD_K)
+            lanes = slice(h * HEAD_V, (h + 1) * HEAD_V)
+            at = 2 * key_cols + h * HEAD_V
+            values_now = mix[b : b + 1, at : at + HEAD_V]
+            new = retained[:, lanes] * past[b, h] + keys_now[entries, b : b + 1] * values_now
+            new_state[b, h] = new
+            retrieved[b : b + 1, lanes] = jnp.sum(
+                queries[entries, b : b + 1] * new, axis=0, keepdims=True
+            )
+    for h in range(local_heads):
+        lanes = slice(h * HEAD_V, (h + 1) * HEAD_V)
+        at = 2 * key_cols + value_cols + h * HEAD_V
+        gate = mix[:, at : at + HEAD_V]
+        found = retrieved[:, lanes]
+        off = found - jnp.mean(found, axis=1, keepdims=True)
+        variance = jnp.mean(off * off, axis=1, keepdims=True)
+        normed = off * lax.rsqrt(variance + EPS_GROUP) * head_gain[:, lanes]
+        heads[:, lanes] = (gate / (1.0 + jnp.exp(-gate)) * normed).astype(BF16)
+
+
+def retain(mix, past_state, head_gain):
     row_count, local_heads = past_state.shape[:2]
-    queries = mix[:, :key_cols]
-    keys_now = mix[:, key_cols : 2 * key_cols]
-    values_now = mix[:, 2 * key_cols : 2 * key_cols + value_cols]
-    gate_now = mix[:, 2 * key_cols + value_cols :]
-    queries = rotate(queries.reshape(row_count, local_heads, HEAD_K)) * HEAD_K ** (-0.5)
-    keys_now = rotate(keys_now.reshape(row_count, local_heads, HEAD_K))
-    values_now = values_now.reshape(row_count, local_heads, HEAD_V)
+    half = HEAD_K // 2
+    frequency = ROPE_BASE ** (-jnp.arange(half, dtype=F32) / half)
+    angles = POS * frequency
+    sine_part = jnp.sin(angles)
+    cosine = jnp.tile(jnp.cos(angles), 2 * local_heads)[None]
+    sine = jnp.tile(jnp.concatenate([-sine_part, sine_part]), local_heads)[None]
     head_level = (lax.axis_index("tp") * local_heads + jnp.arange(local_heads)).astype(F32)
-    retained = 1.0 - jnp.exp2(-5.0 - 16.0 * head_level / (HEADS - 1))
-    new_state = (
-        retained[None, :, None, None] * past_state
-        + keys_now[:, :, :, None] * values_now[:, :, None, :]
-    )
-    retrieved = jnp.einsum("bhk,bhkv->bhv", queries, new_state, precision=lax.Precision.HIGHEST)
-    head_mean = jnp.mean(retrieved, axis=-1, keepdims=True)
-    variance = jnp.mean(jnp.square(retrieved - head_mean), axis=-1, keepdims=True)
-    normed = ((retrieved - head_mean) * lax.rsqrt(variance + EPS_GROUP)).reshape(
-        row_count, local_heads * HEAD_V
-    )
-    return (jax.nn.silu(gate_now) * (normed * head_gain)).astype(BF16), new_state
+    retained = jnp.repeat(1.0 - jnp.exp2(-5.0 - 16.0 * head_level / (HEADS - 1)), HEAD_V)[None]
+    block = 8
+    state = pl.BlockSpec((block,) + past_state.shape[1:], lambda i: (i, 0, 0, 0))
+
+    def rows(width):
+        return pl.BlockSpec((block, width), lambda i: (i, 0))
+
+    def whole(array):
+        return pl.BlockSpec(array.shape, lambda i: (0, 0))
+
+    value_cols = local_heads * HEAD_V
+    gain = head_gain[None]
+    return pl.pallas_call(
+        retain_kernel,
+        grid=(row_count // block,),
+        out_shape=(
+            jax.ShapeDtypeStruct((row_count, value_cols), BF16),
+            jax.ShapeDtypeStruct(past_state.shape, F32),
+        ),
+        in_specs=[rows(mix.shape[1]), state]
+        + [whole(array) for array in (cosine, sine, retained, gain)],
+        out_specs=(rows(value_cols), state),
+        scratch_shapes=[pltpu.VMEM((block, value_cols), F32)],
+        compiler_params=pltpu.CompilerParams(vmem_limit_bytes=STATE_MIB * MIB),
+        cost_estimate=pl.CostEstimate(
+            flops=5 * past_state.size, bytes_accessed=8 * past_state.size, transcendentals=0
+        ),
+    )(mix, past_state, cosine, sine, retained, gain)
 
 
 def fused_shards(
@@ -653,10 +766,9 @@
         + branches
         + project_scratch(shape, rows, mix_cols // (2 * LANES)),
         0,
-    )
-    heads, new_state = retain(
-        mix, past_state, head_gain, query_weight.shape[1], value_weight.shape[1]
-    )
+        FIRST_MIB,
+    )
+    heads, new_state = retain(mix, past_state, head_gain)
     mixed = call(
         last_kernel,
         shape,
@@ -671,6 +783,7 @@
         + hidden
         + branches * 2,
         1,
+        LAST_MIB,
     )
     return mixed, new_state
 
@@ -680,7 +793,7 @@
     tokens, first_gate, mix_weights = arrays[0], arrays[3], arrays[7:11]
     rows, cols = tokens.shape
     whole_tiles = (
-        groups > 1
+        groups == 4
         and width % 4 == 0
         and cols % LANES == 0
         and rows % (16 * groups) == 0

time: 158 us -> 142 us (0.90)
  other arithmetic: 7.67 us -> 0.19 us
  matrix products: 7.33 us -> 0 us
  local copies, waits for them, and re-layouts: 7.11 us -> 3.34 us
  Pallas kernels: 135 us -> 138 us
    pallas_call x0 -> x1, Pallas kernels: none -> 8.82 us  [retain(): pl.pallas_call(retain_kernel, grid=(row_count // block,), out_shape=(jax....]
    dot_general x1 -> x0, matrix products: 7.33 us -> none  [retain(): jnp.einsum('bhk,bhkv->bhv', queries, new_state, precision=lax.Precision.H...]
    pallas_call x2, Pallas kernels: 135 us -> 129 us  [call(): pl.pallas_call(lambda *refs: kernel(shape, *refs), name=kernel.__name__,...]
    add x1 -> x0, other arithmetic: 5.31 us -> none  [retain(): retained[None, :, None, None] * past_state]
    slice x2 -> x0, local copies, waits for them, and re-layouts: 1.8 us -> none  [the longest x1 0.91 us: retain(): values_now = mix[:, 2 * key_cols:2 * key_cols + value_cols]]
    unnamed x5 -> x9, local copies, waits for them, and re-layouts: 4.87 us -> 3.1 us
    convert_element_type x1 -> x0, other arithmetic: 1.58 us -> none  [retain(): (jax.nn.silu(gate_now) * (normed * head_gain)).astype(BF16)]
where the time goes in v2:
time: 142 us
  Pallas kernels  138 us (97%)
  local copies, waits for them, and re-layouts  3.34 us (2%)
    pallas_call x2, Pallas kernels, call(): pl.pallas_call(lambda *refs: kernel(shape, *refs), name=kernel.__name__,...  129 us
    pallas_call x1, Pallas kernels, retain(): pl.pallas_call(retain_kernel, grid=(row_count // block,), out_shape=(jax....  8.82 us
    unnamed x9, local copies, waits for them, and re-layouts  3.1 us

profile of v2, /device:TPU:0, one launch (start us, length us, event | category | flops | bytes accessed | tf_op | source)
XLA Modules:
  0.0 142.0 jit_solution(306421295513053526)
XLA Ops:
  0.7 0.1 fusion
  0.8 0.1 pad_maximum_fusion
  0.8 0.1 broadcast_in_dim_tile.7.sine
  0.9 0.1 broadcast_in_dim.17
  1.0 0.1 broadcast_in_dim_tile.6.cosine
  1.1 0.0 copy-start
  1.1 0.0 copy-start.2
  1.1 69.7 %first_kernel.1 = (bf16[256,128]{1,0:T(8,128)(2,1)}, f32[64,1536]{1,0:T(8,128)}) custom-call(bf16[256,128]{1,0:T(8,128)(2,1)} %refs_0_.1, f32[1,1024]{1,0:T(1,128)} %bitcast.7, f32[1,1024]{1,0:T(1,128)} %bitcast.8, bf16[1024,1408]{1,0:T(8,128)(2,1)} %refs_3_.2, bf16[1024,1408]{1,0:T(8,128)(2,1)} %refs_4_.2, bf16[1408,1024]{1,0:T(8,128)(2,1)} %refs_5_.2, ...), custom_call_target="tpu_custom_call" | custom-call | flops 60000002048 | bytes 100000000 | tf_op jit(solution)/shard_map/first_kernel/pallas_call | solution.py:632
  70.8 0.0 copy-done
  70.8 0.0 copy-done.2
  70.8 0.0 copy-start.1
  70.8 1.0 copy-done.1
  71.8 8.8 %shard_map.176 = (bf16[64,512]{1,0:T(8,128)(2,1)S(1)}, f32[64,4,64,128]{3,2,1,0:T(8,128)}) custom-call(f32[64,1536]{1,0:T(8,128)S(1)} %copy-done.1, f32[64,4,64,128]{3,2,1,0:T(8,128)S(1)} %copy-done, f32[1,256]{1,0:T(1,128)S(1)} %broadcast_in_dim_tile.6.cosine, f32[1,256]{1,0:T(1,128)S(1)} %broadcast_in_dim_tile.7.sine, f32[1,512]{1,0:T(1,128)S(1)} %bitcast.5, ...), custom_call_target="tpu_custom_call" | custom-call | flops 10485760 | bytes 16777216 | tf_op jit(solution)/shard_map/pallas_call | solution.py:708
  80.6 0.0 copy-start.3
  80.7 0.6 copy-done.3
  81.3 59.3 %last_kernel.1 = bf16[256,128]{1,0:T(8,128)(2,1)} custom-call(bf16[64,512]{1,0:T(8,128)(2,1)} %copy-done.3, bf16[256,128]{1,0:T(8,128)(2,1)} %get-tuple-element.8.refs_1_, f32[1,1024]{1,0:T(1,128)} %bitcast.9, bf16[512,1024]{1,0:T(8,128)(2,1)} %refs_3_.3, bf16[1024,1408]{1,0:T(8,128)(2,1)} %refs_4_.3, bf16[1024,1408]{1,0:T(8,128)(2,1)} %refs_5_.3, ...), custom_call_target="tpu_custom_call" | custom-call | flops 60000002048 | bytes 100000000 | tf_op jit(solution)/shard_map/last_kernel/pallas_call | solution.py:632
  140.6 1.5 %copy.20 = bf16[256,128]{1,0:T(8,128)(2,1)} copy(bf16[256,128]{1,0:T(8,128)(2,1)} %last_kernel.1) | data formatting | bytes 131072
  (4 shorter events, 0.1 us)
Async XLA Ops:
  1.1 69.7 %copy-start = (f32[64,4,64,128]{3,2,1,0:T(8,128)S(1)}, f32[64,4,64,128]{3,2,1,0:T(8,128)}, u32[]{:S(2)}) copy-start(f32[64,4,64,128]{3,2,1,0:T(8,128)} %past.1) | copy-start | bytes 25165828
  1.1 69.7 %copy-start.2 = (f32[512]{0:T(512)S(1)}, f32[512]{0:T(512)}, u32[]{:S(2)}) copy-start(f32[512]{0:T(512)} %param.28) | copy-start | bytes 6148
  70.8 1.0 copy-start.1
  80.6 0.6 copy-start.3
